TPU v7x, 32 devices: a whole 2x2x4 slice. The times are simulated.
32 devices in a mesh: sp: 4 (over z), fs: 4 (over y, core), tp: 2 (over x).
Axes of the slice: x: 2, y: 2, z: 4, core: 2. Of those that a mesh axis runs over, the one named last changes fastest.
Arguments:
- tokens: bfloat16 [4, 4096, 2048], P('fs', 'sp', 'tp'), may hold values from -8 to 8
- norm_gain: float32 [2048], replicated, may hold values from 0.1 to 1.9
- w_query: bfloat16 [2048, 1024], P(('sp', 'fs'), 'tp'), may hold values from -4 to 4
- w_key: bfloat16 [2048, 512], P(('sp', 'fs'), 'tp'), may hold values from -0.16 to 0.16
- w_value: bfloat16 [2048, 512], P(('sp', 'fs'), 'tp'), may hold values from -0.125 to 0.125
- w_conv_in: bfloat16 [2048, 1024], P(('sp', 'fs'), 'tp'), may hold values from -0.125 to 0.125
- w_conv_b: bfloat16 [2048, 1024], P(('sp', 'fs'), 'tp'), may hold values from -0.125 to 0.125
- w_conv_c: bfloat16 [2048, 1024], P(('sp', 'fs'), 'tp'), may hold values from -0.125 to 0.125
- conv_taps: bfloat16 [3, 1024], P(None, 'tp'), may hold values from -3.5 to 3.5
- sink_logits: float32 [16], P('tp'), may hold values from 1 to 5
- w_attn_out: bfloat16 [1024, 2048], P('tp', ('sp', 'fs')), may hold values from -0.375 to 0.375
- w_conv_out: bfloat16 [1024, 2048], P('tp', ('sp', 'fs')), may hold values from -0.125 to 0.125
Outputs:
- mixed: bfloat16 [4, 4096, 2048], P('fs', ('sp', 'tp'))
All inputs are finite; a program needn't handle non-finite values.
Results may differ from a plain program's by a relative error of at most 0.02.
Values may be sent and summed in bfloat16 or wider, within the bound.
No kernel may reach another device: no remote copies, remote signals or barrier semaphores. Data moves between devices by JAX's collectives and lax.ppermute only.
A program may use at most 128 MiB of HBM per device.

v0:
```python
import jax
import jax.numpy as jnp
from jax import lax
from jax.sharding import PartitionSpec as P

HEADS = 16
HEAD = 64
WINDOW = 128


def shifted(block, axis, distance):
    devices = range(lax.axis_size(axis))
    route = [(i - distance, i) for i in devices if i - distance in devices]
    return lax.ppermute(block, axis, route)


def norm_rows(tokens, norm_gain):
    values = tokens.astype(jnp.float32)
    average = jnp.mean(values, axis=-1, keepdims=True)
    centred = values - average
    variance = jnp.mean(centred * centred, axis=-1, keepdims=True)
    return (centred * lax.rsqrt(variance + 1e-05) * norm_gain).astype(jnp.bfloat16)


def attend(queries, keys_values, earlier_rows, sink_logits, head_base, row_base):
    row_total = queries.shape[0]
    kv_cols = keys_values.shape[1] // 2
    kv_here = kv_cols // HEAD
    heads_here = queries.shape[1] // HEAD
    group = heads_here // kv_here
    keys_all = jnp.concatenate([earlier_rows, keys_values], axis=0)
    block_rows = min(512, row_total)
    head_ids = head_base + jnp.arange(heads_here, dtype=jnp.int32)
    slopes = jnp.exp2(-8.0 * (head_ids + 1).astype(jnp.float32) / HEADS).reshape(kv_here, group)[
        :, :, None, None
    ]
    sinks = sink_logits.reshape(kv_here, group)[:, :, None, None]
    row_ids = jnp.arange(block_rows, dtype=jnp.int32)[:, None]
    col_ids = jnp.arange(block_rows + WINDOW, dtype=jnp.int32)[None, :]
    distance = WINDOW + row_ids - col_ids
    outputs = []
    for block in range(row_total // block_rows):
        first_row = block * block_rows
        query_block = queries[first_row : first_row + block_rows].reshape(
            block_rows, kv_here, group, HEAD
        )
        band = keys_all[first_row : first_row + block_rows + WINDOW]
        band_keys = band[:, :kv_cols].reshape(block_rows + WINDOW, kv_here, HEAD)
        band_values = band[:, kv_cols:].reshape(block_rows + WINDOW, kv_here, HEAD)
        scores = jnp.einsum(
            "qkgd,skd->kgqs", query_block, band_keys, preferred_element_type=jnp.float32
        ) * HEAD ** (-0.5)
        scores = scores - slopes * distance.astype(jnp.float32)
        key_place = row_base + first_row - WINDOW + col_ids
        keep = (distance >= 0) & (distance < WINDOW) & (key_place >= 0)
        scores = jnp.where(keep, scores, -jnp.inf)
        highest = jnp.maximum(jnp.max(scores, axis=-1, keepdims=True), sinks)
        raised = jnp.exp(scores - highest)
        denominator = jnp.sum(raised, axis=-1, keepdims=True) + jnp.exp(sinks - highest)
        weights = (raised / denominator).astype(jnp.bfloat16)
        mixed = jnp.einsum(
            "kgqs,skd->qkgd", weights, band_values, preferred_element_type=jnp.float32
        )
        outputs.append(mixed.astype(jnp.bfloat16).reshape(block_rows, heads_here * HEAD))
    return jnp.concatenate(outputs, axis=0)


def on_device(
    tokens,
    norm_gain,
    w_query,
    w_key,
    w_value,
    w_conv_in,
    w_conv_b,
    w_conv_c,
    conv_taps,
    sink_logits,
    w_attn_out,
    w_conv_out,
):
    gathered = lax.all_gather(tokens, "tp", axis=2, tiled=True)[0]
    normed = norm_rows(gathered, norm_gain)
    row_total = normed.shape[0]
    weight_rows = (
        lax.all_gather(w_query, ("sp", "fs"), axis=0, tiled=True),
        lax.all_gather(w_key, ("sp", "fs"), axis=0, tiled=True),
        lax.all_gather(w_value, ("sp", "fs"), axis=0, tiled=True),
        lax.all_gather(w_conv_in, ("sp", "fs"), axis=0, tiled=True),
        lax.all_gather(w_conv_b, ("sp", "fs"), axis=0, tiled=True),
        lax.all_gather(w_conv_c, ("sp", "fs"), axis=0, tiled=True),
    )
    results = tuple(
        (
            jnp.dot(normed, rows_part, preferred_element_type=jnp.float32)
            for rows_part in weight_rows
        )
    )
    queries, keys, values, inner, gate_b, gate_c = tuple(
        (result.astype(jnp.bfloat16) for result in results)
    )
    product = (gate_c.astype(jnp.float32) * inner.astype(jnp.float32)).astype(jnp.bfloat16)
    keys_values = jnp.concatenate([keys, values], axis=1)
    earlier_kv, earlier_product = shifted(
        (keys_values[row_total - WINDOW :], product[row_total - 2 :]), "sp", 1
    )
    heads_here = queries.shape[1] // HEAD
    head_base = lax.axis_index("tp") * heads_here
    row_base = lax.axis_index("sp") * row_total
    attended = attend(queries, keys_values, earlier_kv, sink_logits, head_base, row_base)
    taps = conv_taps.astype(jnp.float32)
    padded = jnp.concatenate([earlier_product, product], axis=0).astype(jnp.float32)
    filtered = (
        taps[0] * padded[0:row_total]
        + taps[1] * padded[1 : row_total + 1]
        + taps[2] * padded[2 : row_total + 2]
    )
    conv_out = (gate_b.astype(jnp.float32) * filtered).astype(jnp.bfloat16)
    attn_columns, conv_columns = (
        lax.all_gather(w_attn_out, ("sp", "fs"), axis=1, tiled=True),
        lax.all_gather(w_conv_out, ("sp", "fs"), axis=1, tiled=True),
    )
    summed = lax.psum_scatter(
        (
            jnp.dot(attended, attn_columns, preferred_element_type=jnp.float32)
            + jnp.dot(conv_out, conv_columns, preferred_element_type=jnp.float32)
        ).astype(jnp.bfloat16),
        "tp",
        scatter_dimension=0,
        tiled=True,
    )
    return summed[None]


def solution(mesh):
    placed = (
        P("fs", "sp", "tp"),
        P(),
        P(("sp", "fs"), "tp"),
        P(("sp", "fs"), "tp"),
        P(("sp", "fs"), "tp"),
        P(("sp", "fs"), "tp"),
        P(("sp", "fs"), "tp"),
        P(("sp", "fs"), "tp"),
        P(None, "tp"),
        P("tp"),
        P("tp", ("sp", "fs")),
        P("tp", ("sp", "fs")),
    )
    return jax.shard_map(
        on_device,
        mesh=mesh,
        in_specs=placed,
        out_specs=P("fs", ("sp", "tp"), None),
        check_vma=False,
    )
```

profile of v0, /device:TPU:0, one launch (start us, length us, event | category | flops | bytes accessed | tf_op | source)
XLA Modules:
  0.0 474.1 jit_solution(1467473243379715403)
XLA Ops:
  6.5 0.7 all-gather.10.cloned.1.call-update
  7.3 0.7 all-gather.14.cloned.1.call-update
  10.5 0.7 all-gather.18.cloned.1.call-update
  13.6 54.7 %all-gather.10.cloned.1.call-done = bf16[1,1024,2048]{2,1,0:T(8,128)(2,1)} async-done(((bf16[1,1024,1024]{2,1,0:T(8,128)(2,1)}), bf16[1,1024,2048]{2,1,0:T(8,128)(2,1)}) %all-gather.10.cloned.1.call-update) | async-done | bytes 4194320 | tf_op jit(solution)/shard_map/all_gather | solution.py:82
  68.4 3.0 convert_reduce_fusion
  71.8 1.2 fusion.7
  73.1 2.9 fusion.9
  76.0 32.4 %all-gather.14.cloned.1.call-done = bf16[2048,256]{1,0:T(8,128)(2,1)} async-done(((bf16[128,256]{1,0:T(8,128)(2,1)}), bf16[2048,256]{1,0:T(8,128)(2,1)}) %all-gather.14.cloned.1.call-update) | async-done | bytes 1048592 | tf_op jit(solution)/shard_map/all_gather | solution.py:88
  108.4 3.8 convolution_convert_fusion.4
  112.2 35.3 %all-gather.12.cloned.1.call-done = bf16[2048,256]{1,0:T(8,128)(2,1)} async-done(((bf16[128,256]{1,0:T(8,128)(2,1)}), bf16[2048,256]{1,0:T(8,128)(2,1)}) %all-gather.12.cloned.1.call-update) | async-done | bytes 1048592 | tf_op jit(solution)/shard_map/all_gather | solution.py:87
  147.5 3.8 convolution_convert_fusion.5
  151.3 2.4 collective-permute-start
  153.7 36.2 %all-gather.24.cloned.1.call-done = bf16[2048,512]{1,0:T(8,128)(2,1)} async-done(((bf16[128,512]{1,0:T(8,128)(2,1)}), bf16[2048,512]{1,0:T(8,128)(2,1)}) %all-gather.24.cloned.1.call-update) | async-done | bytes 2097168 | tf_op jit(solution)/shard_map/all_gather | solution.py:89
  189.9 6.2 %convolution_convert_fusion = bf16[1024,512]{1,0:T(8,128)(2,1)} fusion(bf16[1024,2048]{1,0:T(8,128)(2,1)} %fusion.9, bf16[2048,512]{1,0:T(8,128)(2,1)} %all-gather.24.cloned.1.call-done), kind=kOutput, calls=%fused_computation.31 | convolution fusion | flops 2148007936 | bytes 7340032 | tf_op jit(solution)/shard_map/dot_general | solution.py:95
  196.1 36.1 %all-gather.22.cloned.1.call-done = bf16[2048,512]{1,0:T(8,128)(2,1)} async-done(((bf16[128,512]{1,0:T(8,128)(2,1)}), bf16[2048,512]{1,0:T(8,128)(2,1)}) %all-gather.22.cloned.1.call-update) | async-done | bytes 2097168 | tf_op jit(solution)/shard_map/all_gather | solution.py:91
  232.1 5.5 %multiply_convert_fusion = bf16[1024,512]{1,0:T(8,128)(2,1)S(1)} fusion(bf16[1024,512]{1,0:T(8,128)(2,1)} %convolution_convert_fusion, bf16[1024,2048]{1,0:T(8,128)(2,1)} %fusion.9, bf16[2048,512]{1,0:T(8,128)(2,1)} %all-gather.22.cloned.1.call-done), kind=kOutput, calls=%fused_computation.30 | convolution fusion | flops 2150105088 | bytes 8388608 | tf_op jit(solution)/shard_map/dot_general | solution.py:95
  237.6 1.0 copy-done.2
  238.6 2.4 collective-permute-start.1
  241.0 33.4 %all-gather.16.cloned.1.call-done = bf16[2048,512]{1,0:T(8,128)(2,1)} async-done(((bf16[128,512]{1,0:T(8,128)(2,1)}), bf16[2048,512]{1,0:T(8,128)(2,1)}) %all-gather.16.cloned.1.call-update) | async-done | bytes 2097168 | tf_op jit(solution)/shard_map/all_gather | solution.py:86
  274.4 5.3 %convolution_convert_fusion.3 = bf16[1024,512]{0,1:T(8,128)(2,1)S(1)} fusion(bf16[1024,2048]{1,0:T(8,128)(2,1)} %fusion.9, bf16[2048,512]{1,0:T(8,128)(2,1)} %all-gather.16.cloned.1.call-done), kind=kOutput, calls=%fused_computation.34 | convolution fusion | flops 2148007936 | bytes 7340032 | tf_op jit(solution)/shard_map/dot_general | solution.py:95
  279.8 1.6 maximum_convert_fusion
  281.6 5.8 %fusion.11 = (f32[4,2,512]{2,1,0:T(2,128)S(1)}, f32[4,640,512,2]{2,1,3,0:T(8,128)}) fusion(f32[512,640]{0,1:T(8,128)S(1)} %fusion.18, f32[4,2]{1,0:T(4,128)S(1)} %multiply_exponential_fusion, pred[512,640]{0,1:T(8,128)(4,1)S(1)} %get-tuple-element.19, bf16[640,4,64,1]{0,2,3,1:T(8,128)(2,1)S(1)} %bitcast.93, bf16[512,4,2,64]{0,3,2,1:T(8,128)(2,1)S(1)} %bitcast.89), kind=kOutput, calls=%fused_computation.20 | convolution fusion | flops 348647424 | bytes 12992544 | tf_op jit(solution)/shard_map/qkgd,skd->kgqs/dot_general | solution.py:50
  287.4 8.4 %fusion.2 = (f32[4,2,512]{2,1,0:T(2,128)S(1)}, f32[4,2,512]{2,1,0:T(2,128)S(1)}, f32[4,640,512,2]{2,1,3,0:T(8,128)S(1)}) fusion(f32[4,640,512,2]{2,1,3,0:T(8,128)} %get-tuple-element.21, f32[4,2,512]{2,1,0:T(2,128)S(1)} %broadcast_maximum_fusion.1, f32[512,640]{0,1:T(8,128)S(1)} %fusion.18, f32[4,2]{1,0:T(4,128)S(1)} %multiply_exponential_fusion, ...), kind=kOutput, calls=%fused_computation.10 | convolution fusion | flops 361750528 | bytes 23838752 | tf_op jit(solution)/shard_map/qkgd,skd->kgqs/dot_general | solution.py:50
  295.9 2.9 fusion.3
  298.9 8.0 %fusion.23 = bf16[4,64,2,512]{3,1,2,0:T(8,128)(2,1)S(1)} fusion(bf16[640,4,64,1]{0,2,3,1:T(8,128)(2,1)S(1)} %bitcast.91, f32[4,640,512,2]{2,1,3,0:T(8,128)} %get-tuple-element.21, f32[4,2,512]{2,1,0:T(2,128)S(1)} %get-tuple-element.16, f32[4,2,512]{2,1,0:T(2,128)S(1)} %broadcast_maximum_fusion.1, f32[512,640]{0,1:T(8,128)S(1)} %fusion.18, ...), kind=kOutput, calls=%fused_computation.43 | convolution fusion | flops 354156544 | bytes 13008928 | tf_op jit(solution)/shard_map/kgqs,skd->qkgd/dot_general | solution.py:61
  306.9 4.0 fusion.22
  310.9 5.4 %all-gather.18.cloned.1.call-done = bf16[512,2048]{1,0:T(8,128)(2,1)} async-done(((bf16[512,128]{1,0:T(8,128)(2,1)}), bf16[512,2048]{1,0:T(8,128)(2,1)}) %all-gather.18.cloned.1.call-update) | async-done | bytes 2097168 | tf_op jit(solution)/shard_map/all_gather | solution.py:120
  316.3 7.4 %fusion.24 = f32[1024,2048]{1,0:T(8,128)} fusion(bf16[512,2048]{1,0:T(8,128)(2,1)} %all-gather.18.cloned.1.call-done, bf16[512,512]{0,1:T(8,128)(2,1)S(1)} %bitcast.98, bf16[512,512]{0,1:T(8,128)(2,1)S(1)} %bitcast.97), kind=kOutput, calls=%fused_computation.45 | convolution fusion | flops 2149580800 | bytes 11534336 | tf_op jit(solution)/shard_map/dot_general | solution.py:125
  323.7 35.3 %all-gather.20.cloned.1.call-done = bf16[2048,512]{1,0:T(8,128)(2,1)} async-done(((bf16[128,512]{1,0:T(8,128)(2,1)}), bf16[2048,512]{1,0:T(8,128)(2,1)}) %all-gather.20.cloned.1.call-update) | async-done | bytes 2097168 | tf_op jit(solution)/shard_map/all_gather | solution.py:90
  359.0 42.0 %all-gather.26.cloned.1.call-done = bf16[512,2048]{1,0:T(8,128)(2,1)} async-done(((bf16[512,128]{1,0:T(8,128)(2,1)}), bf16[512,2048]{1,0:T(8,128)(2,1)}) %all-gather.26.cloned.1.call-update) | async-done | bytes 2097168 | tf_op jit(solution)/shard_map/all_gather | solution.py:121
  401.0 12.6 %add_convert_fusion = bf16[1024,2048]{1,0:T(8,128)(2,1)} fusion(f32[1024,2048]{1,0:T(8,128)} %fusion.24, bf16[512,2048]{1,0:T(8,128)(2,1)} %all-gather.26.cloned.1.call-done, f32[1026,512]{1,0:T(8,128)S(1)} %copy-done.1, bf16[1024,2048]{1,0:T(8,128)(2,1)} %fusion.9, bf16[2048,512]{1,0:T(8,128)(2,1)} %all-gather.20.cloned.1.call-done, f32[512]{0:T(512)S(1)} %bitcast.96, ...), kind=kOutput, calls=%fused_computation.18 | convolution fusion | flops 4303880192 | bytes 27269120 | tf_op jit(solution)/shard_map/dot_general | solution.py:126
  413.6 53.6 %reduce-scatter.2.cloned.1.call-done = bf16[512,2048]{1,0:T(8,128)(2,1)} async-done(((bf16[1024,2048]{1,0:T(8,128)(2,1)}), bf16[512,2048]{1,0:T(8,128)(2,1)}) %reduce-scatter.2.cloned.1.call-update) | async-done | bytes 2097168 | tf_op jit(solution)/shard_map/reduce_scatter | solution.py:123
  (48 shorter events, 5.8 us)
Async XLA Ops:
  6.5 6.5 %copy-start.6 = (f32[8]{0:T(128)S(1)}, f32[8]{0:T(128)}, u32[]{:S(2)}) copy-start(f32[8]{0:T(128)} %param.21) | copy-start | bytes 100
  6.5 6.5 %copy-start.4 = (bf16[3,512]{1,0:T(4,128)(2,1)S(1)}, bf16[3,512]{1,0:T(4,128)(2,1)}, u32[]{:S(2)}) copy-start(bf16[3,512]{1,0:T(4,128)(2,1)} %param.20) | copy-start | bytes 9220
  6.5 61.8 %all-gather.10.cloned.1.call-start = ((), (), s32[]{:S(2)}) async-start(), calls=%async_computation.1 | async-start | bytes 6291456 | tf_op jit(solution)/shard_map/all_gather | solution.py:82
  7.3 101.2 %all-gather.14.cloned.1.call-start = ((), (), s32[]{:S(2)}) async-start(), calls=%async_computation.3 | async-start | bytes 1114112 | tf_op jit(solution)/shard_map/all_gather | solution.py:88
  8.0 139.4 %all-gather.12.cloned.1.call-start = ((), (), s32[]{:S(2)}) async-start(), calls=%async_computation.2 | async-start | bytes 1114112 | tf_op jit(solution)/shard_map/all_gather | solution.py:87
  8.7 181.2 %all-gather.24.cloned.1.call-start = ((), (), s32[]{:S(2)}) async-start(), calls=%async_computation.8 | async-start | bytes 2228224 | tf_op jit(solution)/shard_map/all_gather | solution.py:89
  9.3 222.8 %all-gather.22.cloned.1.call-start = ((), (), s32[]{:S(2)}) async-start(), calls=%async_computation.7 | async-start | bytes 2228224 | tf_op jit(solution)/shard_map/all_gather | solution.py:91
  9.9 264.5 %all-gather.16.cloned.1.call-start = ((), (), s32[]{:S(2)}) async-start(), calls=%async_computation.4 | async-start | bytes 2228224 | tf_op jit(solution)/shard_map/all_gather | solution.py:86
  10.5 305.8 %all-gather.18.cloned.1.call-start = ((), (), s32[]{:S(2)}) async-start(), calls=%async_computation.5 | async-start | bytes 2228224 | tf_op jit(solution)/shard_map/all_gather | solution.py:120
  11.2 347.8 %all-gather.20.cloned.1.call-start = ((), (), s32[]{:S(2)}) async-start(), calls=%async_computation.6 | async-start | bytes 2228224 | tf_op jit(solution)/shard_map/all_gather | solution.py:90
  12.0 389.0 %all-gather.26.cloned.1.call-start = ((), (), s32[]{:S(2)}) async-start(), calls=%async_computation.9 | async-start | bytes 2228224 | tf_op jit(solution)/shard_map/all_gather | solution.py:121
  12.7 454.5 %reduce-scatter.2.cloned.1.call-start = ((), (), s32[]{:S(2)}) async-start(), calls=%async_computation.10 | async-start | bytes 6291456 | tf_op jit(solution)/shard_map/reduce_scatter | solution.py:123
  13.6 59.4 %copy-start.5 = (f32[2048]{0:T(1024)S(1)}, f32[2048]{0:T(1024)}, u32[]{:S(2)}) copy-start(f32[2048]{0:T(1024)} %param.13) | copy-start | bytes 24580
  68.4 3.4 copy-start
  151.3 130.1 %collective-permute-start = (bf16[128,512]{0,1:T(8,128)(2,1)S(1)}, bf16[128,512]{0,1:T(8,128)(2,1)S(1)}, u32[]{:S(2)}, u32[]{:S(2)}) collective-permute-start(bf16[128,512]{0,1:T(8,128)(2,1)S(1)} %pad_maximum_fusion.3), channel_id=1, source_target_pairs={{0,8},{8,16},{16,24},{1,9},{9,17},{17,25},{2,10},{10,18},{18,26},{... | collective-permute-start | bytes 393224 | tf_op jit(solution)/shard_map/ppermute | solution.py:14
  237.6 1.0 copy-start.2
  238.6 41.2 %collective-permute-start.1 = (bf16[2,512]{1,0:T(2,128)(2,1)S(1)}, bf16[2,512]{1,0:T(2,128)(2,1)S(1)}, u32[]{:S(2)}, u32[]{:S(2)}) collective-permute-start(bf16[2,512]{1,0:T(2,128)(2,1)S(1)} %slice.69), channel_id=1, source_target_pairs={{0,8},{8,16},{16,24},{1,9},{9,17},{17,25},{2,10},{10,18},{18,26},{... | collective-permute-start | bytes 6152 | tf_op jit(solution)/shard_map/ppermute | solution.py:14
  274.4 5.4 %copy-start.3 = (bf16[1024,512]{1,0:T(8,128)(2,1)S(1)}, bf16[1024,512]{1,0:T(8,128)(2,1)}, u32[]{:S(2)}) copy-start(bf16[1024,512]{1,0:T(8,128)(2,1)} %copy-done.2) | copy-start | bytes 3145732
  316.3 84.7 %copy-start.1 = (f32[1026,512]{1,0:T(8,128)S(1)}, f32[1026,512]{1,0:T(8,128)}, u32[]{:S(2)}) copy-start(f32[1026,512]{1,0:T(8,128)} %maximum_convert_fusion) | copy-start | bytes 6303748
Sparse Core Ops, SparseCore 0:
  8.9 59.4 all-gather.9
  70.5 37.8 all-gather.13
  110.6 36.8 all-gather.11
  149.5 40.4 all-gather.23
  191.9 40.1 all-gather.21
  234.2 40.1 all-gather.15
  276.5 39.7 all-gather.17
  318.5 40.5 all-gather.19
  361.2 39.7 all-gather.25
  413.7 53.4 reduce-scatter.1
where the time goes:
time: 474 us
  waiting for transfers between devices  370 us (78%)
  matrix products  70.7 us (15%)
  between operations  13.7 us (3%)
  other arithmetic  12.8 us (3%)
  starting transfers between devices  5.16 us (1%)
    all_gather x1, waiting for transfers between devices, on_device(): gathered = lax.all_gather(tokens, 'tp', axis=2, tiled=True)[0]  54.7 us
    reduce_scatter x1, waiting for transfers between devices, on_device(): lax.psum_scatter((jnp.dot(attended, attn_columns, preferred_element_type=...  53.6 us
    all_gather x1, waiting for transfers between devices, on_device(): lax.all_gather(w_conv_out, ('sp', 'fs'), axis=1, tiled=True)  42 us
    all_gather x1, waiting for transfers between devices, on_device(): lax.all_gather(w_conv_in, ('sp', 'fs'), axis=0, tiled=True)  36.2 us
    all_gather x1, waiting for transfers between devices, on_device(): lax.all_gather(w_conv_c, ('sp', 'fs'), axis=0, tiled=True)  36.1 us
    all_gather x1, waiting for transfers between devices, on_device(): lax.all_gather(w_conv_b, ('sp', 'fs'), axis=0, tiled=True)  35.3 us
    all_gather x1, waiting for transfers between devices, on_device(): lax.all_gather(w_key, ('sp', 'fs'), axis=0, tiled=True)  35.3 us
    all_gather x1, waiting for transfers between devices, on_device(): lax.all_gather(w_query, ('sp', 'fs'), axis=0, tiled=True)  33.4 us
  transfers between devices with their start and end apart: 12, of which 10 were waited for; matrix products, arithmetic and copies ran while one was open for 15% of the time, Pallas kernels for 0%

commit v1 on v0

v1 whole, which is shorter than its diff:
```python
import jax
import jax.numpy as jnp
from jax import lax
from jax.sharding import PartitionSpec as P

HEADS = 16
HEAD = 64
WINDOW = 128


def shifted(block, axis, distance):
    devices = range(lax.axis_size(axis))
    route = [(i - distance, i) for i in devices if i - distance in devices]
    return lax.ppermute(block, axis, route)


def norm_rows(tokens, norm_gain):
    values = tokens.astype(jnp.float32)
    average = jnp.mean(values, axis=-1, keepdims=True)
    centred = values - average
    variance = jnp.mean(centred * centred, axis=-1, keepdims=True)
    return (centred * lax.rsqrt(variance + 1e-05) * norm_gain).astype(jnp.bfloat16)


def attend_block(queries, band, sink_logits, head_base, row_base):
    block_rows = queries.shape[0]
    kv_cols = band.shape[1] // 2
    kv_here = kv_cols // HEAD
    heads_here = queries.shape[1] // HEAD
    group = heads_here // kv_here
    head_ids = head_base + jnp.arange(heads_here, dtype=jnp.int32)
    slopes = jnp.exp2(-8.0 * (head_ids + 1).astype(jnp.float32) / HEADS).reshape(kv_here, group)[
        :, :, None, None
    ]
    sinks = sink_logits.reshape(kv_here, group)[:, :, None, None]
    row_ids = jnp.arange(block_rows, dtype=jnp.int32)[:, None]
    col_ids = jnp.arange(block_rows + WINDOW, dtype=jnp.int32)[None, :]
    distance = WINDOW + row_ids - col_ids
    query_block = queries.reshape(block_rows, kv_here, group, HEAD)
    band_keys = band[:, :kv_cols].reshape(block_rows + WINDOW, kv_here, HEAD)
    band_values = band[:, kv_cols:].reshape(block_rows + WINDOW, kv_here, HEAD)
    scores = jnp.einsum(
        "qkgd,skd->kgqs", query_block, band_keys, preferred_element_type=jnp.float32
    ) * HEAD ** (-0.5)
    scores = scores - slopes * distance.astype(jnp.float32)
    key_place = row_base - WINDOW + col_ids
    keep = (distance >= 0) & (distance < WINDOW) & (key_place >= 0)
    scores = jnp.where(keep, scores, -jnp.inf)
    highest = jnp.maximum(jnp.max(scores, axis=-1, keepdims=True), sinks)
    raised = jnp.exp(scores - highest)
    denominator = jnp.sum(raised, axis=-1, keepdims=True) + jnp.exp(sinks - highest)
    weights = (raised / denominator).astype(jnp.bfloat16)
    mixed = jnp.einsum("kgqs,skd->qkgd", weights, band_values, preferred_element_type=jnp.float32)
    return mixed.astype(jnp.bfloat16).reshape(block_rows, heads_here * HEAD)


def gather_features(block, axis):
    size = lax.axis_size(axis)
    here = lax.axis_index(axis)
    cols = block.shape[1]
    whole = jnp.zeros((block.shape[0], cols * size), block.dtype)
    whole = lax.dynamic_update_slice(whole, block, (0, here * cols))
    for step in range(1, size):
        other = lax.ppermute(block, axis, [(i, (i + step) % size) for i in range(size)])
        whole = lax.dynamic_update_slice(whole, other, (0, (here - step) % size * cols))
    return whole


def gather_weights(in_part, out_parts):
    in_rows = lax.all_gather(in_part, ("sp", "fs"), axis=0, tiled=True)
    out_part = jnp.concatenate(out_parts, axis=0)
    return in_rows, lax.all_gather(out_part, ("sp", "fs"), axis=1, tiled=True)


def on_device(
    tokens,
    norm_gain,
    w_query,
    w_key,
    w_value,
    w_conv_in,
    w_conv_b,
    w_conv_c,
    conv_taps,
    sink_logits,
    w_attn_out,
    w_conv_out,
):
    ins = (w_key, w_value, w_conv_in, w_conv_c, w_query, w_conv_b)
    in_rows, out_columns = gather_weights(jnp.concatenate(ins, axis=1), (w_attn_out, w_conv_out))
    normed = norm_rows(gather_features(tokens[0], "tp"), norm_gain)
    row_total = normed.shape[0]
    projected = jnp.dot(normed, in_rows, preferred_element_type=jnp.float32).astype(jnp.bfloat16)
    stops = [0]
    for part in ins:
        stops.append(stops[-1] + part.shape[1])
    _, _, inner, gate_c, queries, gate_b = (projected[:, i:j] for i, j in zip(stops, stops[1:]))
    keys_values = projected[:, : stops[2]]
    product = (gate_c.astype(jnp.float32) * inner.astype(jnp.float32)).astype(jnp.bfloat16)
    earlier_kv, earlier_product = shifted(
        (keys_values[row_total - WINDOW :], product[row_total - 2 :]), "sp", 1
    )
    kv_all = jnp.concatenate([earlier_kv, keys_values], axis=0)
    padded = jnp.concatenate([earlier_product, product], axis=0)
    size = lax.axis_size("tp")
    here = lax.axis_index("tp")
    heads_here = queries.shape[1] // HEAD
    row_base = lax.axis_index("sp") * row_total
    taps = conv_taps.astype(jnp.float32)
    rows = row_total // size

    def partial(first):
        attended = attend_block(
            lax.dynamic_slice_in_dim(queries, first, rows, 0),
            lax.dynamic_slice_in_dim(kv_all, first, rows + WINDOW, 0),
            sink_logits,
            here * heads_here,
            row_base + first,
        )
        near = lax.dynamic_slice_in_dim(padded, first, rows + 2, 0).astype(jnp.float32)
        filtered = taps[0] * near[:rows] + taps[1] * near[1 : rows + 1] + taps[2] * near[2:]
        gate = lax.dynamic_slice_in_dim(gate_b, first, rows, 0).astype(jnp.float32)
        conv_out = (gate * filtered).astype(jnp.bfloat16)
        both = jnp.concatenate([attended, conv_out], axis=1)
        return jnp.dot(both, out_columns, preferred_element_type=jnp.float32).astype(jnp.bfloat16)

    arrived = []
    for step in range(1, size):
        piece = partial((here + step) % size * rows)
        piece, queries, kv_all, padded, gate_b = lax.optimization_barrier(
            (piece, queries, kv_all, padded, gate_b)
        )
        arrived.append(lax.ppermute(piece, "tp", [(i, (i + step) % size) for i in range(size)]))
    summed = partial(here * rows).astype(jnp.float32)
    for piece in arrived:
        summed = summed + piece.astype(jnp.float32)
    return summed.astype(jnp.bfloat16)[None]


def solution(mesh):
    placed = (
        P("fs", "sp", "tp"),
        P(),
        P(("sp", "fs"), "tp"),
        P(("sp", "fs"), "tp"),
        P(("sp", "fs"), "tp"),
        P(("sp", "fs"), "tp"),
        P(("sp", "fs"), "tp"),
        P(("sp", "fs"), "tp"),
        P(None, "tp"),
        P("tp"),
        P("tp", ("sp", "fs")),
        P("tp", ("sp", "fs")),
    )
    return jax.shard_map(
        on_device,
        mesh=mesh,
        in_specs=placed,
        out_specs=P("fs", ("sp", "tp"), None),
        check_vma=False,
    )
```

time: 474 us -> 236 us (0.50)
  waiting for transfers between devices: 370 us -> 116 us
  local copies, waits for them, and re-layouts: 1.63 us -> 28.9 us
  matrix products: 70.7 us -> 48.5 us
  starting transfers between devices: 5.16 us -> 10.6 us
  other arithmetic: 12.8 us -> 17.6 us
    all_gather x9 -> x2, waiting for transfers between devices: 311 us -> 41 us  [the longest x1 37.5 us: gather_weights(): in_rows = lax.all_gather(in_part, ('sp', 'fs'), axis=0, tiled=True)]
    ppermute x0 -> x2, waiting for transfers between devices: none -> 75.3 us  [the longest x1 39.6 us: gather_features(): lax.ppermute(block, axis, [(i, (i + step) % size) for i in range(size)])]
    reduce_scatter x1 -> x0, waiting for transfers between devices: 53.6 us -> none  [on_device(): lax.psum_scatter((jnp.dot(attended, attn_columns, preferred_element_type=...]
    dot_general x11 -> x7, matrix products: 70.7 us -> 48.5 us  [the longest x1 15.4 us: on_device(): jnp.dot(normed, in_rows, preferred_element_type=jnp.float32)]
    slice x2 -> x9, local copies, waits for them, and re-layouts: 0.08 us -> 8.33 us  [the longest x2 2.76 us: attend_block(): band_values = band[:, kv_cols:].reshape(block_rows + WINDOW, kv_here, HEAD)]
    unnamed x14 -> x37, local copies, waits for them, and re-layouts: 1.47 us -> 7.52 us
    dynamic_slice x0 -> x4, local copies, waits for them, and re-layouts: none -> 5.81 us  [partial(): lax.dynamic_slice_in_dim(queries, first, rows, 0)]
    unnamed x10 -> x2, waiting for transfers between devices: 5.76 us -> 0.03 us
  transfers between devices with their start and end apart: 12 -> 6, of which waited for: 10 -> 4; matrix products, arithmetic and copies ran while one was open for 15% -> 27% of each run, Pallas kernels for 0% -> 0%
where the time goes in v1:
time: 236 us
  waiting for transfers between devices  116 us (49%)
  matrix products  48.5 us (21%)
  local copies, waits for them, and re-layouts  28.9 us (12%)
  other arithmetic  17.6 us (7%)
  between operations  13.7 us (6%)
  starting transfers between devices  10.6 us (4%)
    ppermute x1, waiting for transfers between devices, gather_features(): lax.ppermute(block, axis, [(i, (i + step) % size) for i in range(size)])  39.6 us
    all_gather x1, waiting for transfers between devices, gather_weights(): in_rows = lax.all_gather(in_part, ('sp', 'fs'), axis=0, tiled=True)  37.5 us
    ppermute x1, waiting for transfers between devices, on_device(): lax.ppermute(piece, 'tp', [(i, (i + step) % size) for i in range(size)])  35.7 us
    dot_general x1, matrix products, on_device(): jnp.dot(normed, in_rows, preferred_element_type=jnp.float32)  15.4 us
    dot_general x2, matrix products, attend_block(): jnp.einsum('kgqs,skd->qkgd', weights, band_values, preferred_element_type...  13.1 us
    dot_general x2, matrix products, partial(): jnp.dot(both, out_columns, preferred_element_type=jnp.float32)  11.4 us
    dot_general x2, matrix products, attend_block(): jnp.einsum('qkgd,skd->kgqs', query_block, band_keys, preferred_element_ty...  8.63 us
    unnamed x37, local copies, waits for them, and re-layouts  7.52 us
  transfers between devices with their start and end apart: 6, of which 4 were waited for; matrix products, arithmetic and copies ran while one was open for 27% of the time, Pallas kernels for 0%

profile of v1, /device:TPU:0, one launch (start us, length us, event | category | flops | bytes accessed | tf_op | source)
XLA Modules:
  0.0 235.7 jit_solution(1735962592657705360)
XLA Ops:
  10.1 1.1 constant_dynamic-update-slice_fusion.1
  13.0 3.0 %collective-permute-start = (bf16[1024,1024]{1,0:T(8,128)(2,1)}, bf16[1024,1024]{1,0:T(8,128)(2,1)}, u32[]{:S(2)}, u32[]{:S(2)}) collective-permute-start(bf16[1024,1024]{1,0:T(8,128)(2,1)} %bitcast.66), channel_id=1, source_target_pairs={{0,1},{1,0},{2,3},{3,2},{4,5},{5,4},{6,7},{7,6},{8,9},{9,8},{10,11... | collective-permute-start | bytes 6291464 | tf_op jit(solution)/shard_map/ppermute | solution.py:64
  16.0 1.7 pad_maximum_fusion.2
  18.5 1.4 fusion.51
  19.9 1.4 fusion.39
  22.3 39.6 %collective-permute-done = bf16[1024,1024]{1,0:T(8,128)(2,1)} collective-permute-done((bf16[1024,1024]{1,0:T(8,128)(2,1)}, bf16[1024,1024]{1,0:T(8,128)(2,1)}, u32[]{:S(2)}, u32[]{:S(2)}) %collective-permute-start) | collective-permute-done | bytes 2097184 | tf_op jit(solution)/shard_map/ppermute | solution.py:64
  62.0 1.9 constant_dynamic-update-slice_fusion.6
  64.5 1.2 fusion.6
  65.8 37.5 %all-gather.3.cloned.1.call-done = bf16[2048,2560]{1,0:T(8,128)(2,1)} async-done(((bf16[128,2560]{1,0:T(8,128)(2,1)}), bf16[2048,2560]{1,0:T(8,128)(2,1)}) %all-gather.3.cloned.1.call-update) | async-done | bytes 10485776 | tf_op jit(solution)/shard_map/all_gather | solution.py:70
  103.3 15.4 %convolution_convert_fusion = bf16[1024,2560]{1,0:T(8,128)(2,1)S(1)} fusion(bf16[2048,2560]{1,0:T(8,128)(2,1)} %all-gather.3.cloned.1.call-done, bf16[1024,2048]{1,0:T(8,128)(2,1)} %copy-done, f32[2048]{0:T(1024)S(1)} %copy-done.15, f32[1024]{0:T(1024)S(1)} %add_rsqrt_fusion, f32[1024]{0:T(1024)S(1)} %broadcast_multiply_fusion), kind=kOutput, calls=%fused_computation.17 | convolution fusion | flops 10750525440 | bytes 19939328 | tf_op jit(solution)/shard_map/dot_general | solution.py:93
  120.3 3.2 %collective-permute-start.2 = (bf16[2,512]{1,0:T(2,128)(2,1)}, bf16[2,512]{1,0:T(2,128)(2,1)}, u32[]{:S(2)}, u32[]{:S(2)}) collective-permute-start(bf16[2,512]{1,0:T(2,128)(2,1)} %slice.93), channel_id=1, source_target_pairs={{0,8},{8,16},{16,24},{1,9},{9,17},{17,25},{2,10},{10,18},{18,26},{... | collective-permute-start | bytes 6152 | tf_op jit(solution)/shard_map/ppermute | solution.py:14
  123.5 2.8 %collective-permute-start.1 = (bf16[128,512]{1,0:T(8,128)(2,1)}, bf16[128,512]{1,0:T(8,128)(2,1)S(1)}, u32[]{:S(2)}, u32[]{:S(2)}) collective-permute-start(bf16[128,512]{1,0:T(8,128)(2,1)} %slice.84), channel_id=1, source_target_pairs={{0,8},{8,16},{16,24},{1,9},{9,17},{17,25},{2,10},{10,18},{18,26},{... | collective-permute-start | bytes 393224 | tf_op jit(solution)/shard_map/ppermute | solution.py:14
  126.4 1.2 fusion.49
  129.4 2.1 copy.23
  131.6 2.2 pad_maximum_fusion.1
  133.8 1.9 fusion.30
  136.8 1.2 copy.22
  137.9 1.9 copy.21
  139.8 4.2 %fusion.10 = (f32[4,2,512]{2,1,0:T(2,128)S(1)}, f32[4,640,512,2]{2,1,3,0:T(8,128)S(1)}) fusion(f32[512,640]{0,1:T(8,128)S(1)} %fusion.18, f32[4,2]{1,0:T(4,128)S(1)} %multiply_exponential_fusion, pred[512,640]{0,1:T(8,128)(4,1)S(1)} %copy-done.10, bf16[640,4,64,1]{0,2,3,1:T(8,128)(2,1)S(1)} %bitcast.73, bf16[512,4,2,64]{0,3,2,1:T(8,128)(2,1)} %bitcast.67), kind=kOutput, calls=%fused_computation.19 | convolution fusion | flops 348647424 | bytes 12992544 | tf_op jit(solution)/shard_map/qkgd,skd->kgqs/dot_general | solution.py:42
  144.1 2.9 %fusion.4 = f32[4,2,512]{2,1,0:T(2,128)S(1)} fusion(f32[4,640,512,2]{2,1,3,0:T(8,128)S(1)} %get-tuple-element.28, f32[4,2,512]{2,1,0:T(2,128)S(1)} %broadcast_maximum_fusion.1, f32[512,640]{0,1:T(8,128)S(1)} %fusion.18, f32[4,2]{1,0:T(4,128)S(1)} %multiply_exponential_fusion, pred[512,640]{0,1:T(8,128)(4,1)S(1)} %copy-done.10), kind=kLoop, calls=%fused_computation.12 | loop fusion | flops 15724544 | bytes 12156960 | tf_op jit(solution)/shard_map/reduce_sum | solution.py:51
  147.2 4.0 %fusion.23 = bf16[4,64,2,512]{3,1,2,0:T(8,128)(2,1)S(1)} fusion(bf16[640,4,64,1]{0,2,3,1:T(8,128)(2,1)S(1)} %bitcast.71, f32[4,640,512,2]{2,1,3,0:T(8,128)S(1)} %get-tuple-element.28, f32[4,2,512]{2,1,0:T(2,128)S(1)} %exponential_add_fusion.1, f32[4,2,512]{2,1,0:T(2,128)S(1)} %broadcast_maximum_fusion.1, f32[512,640]{0,1:T(8,128)S(1)} %fusion.18, ...), kind=kOutput, calls=%fused_computation.40 | convolution fusion | flops 354156544 | bytes 13008928 | tf_op jit(solution)/shard_map/kgqs,skd->qkgd/dot_general | solution.py:53
  152.2 1.1 pad_maximum_fusion
  153.3 3.5 %all-gather.5.cloned.1.call-done = bf16[1024,2048]{1,0:T(8,128)(2,1)} async-done(((bf16[1024,128]{1,0:T(8,128)(2,1)}), bf16[1024,2048]{1,0:T(8,128)(2,1)}) %all-gather.5.cloned.1.call-update) | async-done | bytes 4194320 | tf_op jit(solution)/shard_map/all_gather | solution.py:72
  156.8 6.2 %convolution_convert_fusion.2 = bf16[512,2048]{1,0:T(8,128)(2,1)} fusion(bf16[1024,2048]{1,0:T(8,128)(2,1)} %all-gather.5.cloned.1.call-done, bf16[512,512]{1,0:T(8,128)(2,1)} %fusion.30, bf16[512,512]{1,0:T(8,128)(2,1)} %copy.25), kind=kOutput, calls=%fused_computation.27 | convolution fusion | flops 2150629376 | bytes 7340032 | tf_op jit(solution)/shard_map/dot_general | solution.py:125
  163.8 2.1 copy.28
  166.1 4.4 %fusion.9 = (f32[4,2,512]{2,1,0:T(2,128)S(1)}, f32[4,640,512,2]{2,1,3,0:T(8,128)S(1)}) fusion(f32[512,640]{0,1:T(8,128)S(1)} %fusion.18, f32[4,2]{1,0:T(4,128)S(1)} %multiply_exponential_fusion, pred[512,640]{0,1:T(8,128)(4,1)} %get-tuple-element.25, bf16[640,4,64,1]{0,2,3,1:T(8,128)(2,1)S(1)} %bitcast.74, bf16[512,4,2,64]{0,3,2,1:T(8,128)(2,1)} %bitcast.68), kind=kOutput, calls=%fused_computation.18 | convolution fusion | flops 348647424 | bytes 12992544 | tf_op jit(solution)/shard_map/qkgd,skd->kgqs/dot_general | solution.py:42
  170.6 2.9 %fusion.5 = f32[4,2,512]{2,1,0:T(2,128)S(1)} fusion(f32[4,640,512,2]{2,1,3,0:T(8,128)S(1)} %get-tuple-element.30, f32[4,2,512]{2,1,0:T(2,128)S(1)} %broadcast_maximum_fusion, f32[512,640]{0,1:T(8,128)S(1)} %fusion.18, f32[4,2]{1,0:T(4,128)S(1)} %multiply_exponential_fusion, pred[512,640]{0,1:T(8,128)(4,1)S(1)} %copy-done.9), kind=kLoop, calls=%fused_computation.13 | loop fusion | flops 15724544 | bytes 12156960 | tf_op jit(solution)/shard_map/reduce_sum | solution.py:51
  175.5 1.5 collective-permute-start.3
  177.0 9.1 %fusion.22 = bf16[4,64,2,512]{3,1,2,0:T(8,128)(2,1)} fusion(bf16[640,4,64,1]{0,2,3,1:T(8,128)(2,1)} %bitcast.72, f32[4,640,512,2]{2,1,3,0:T(8,128)} %copy-done.1, f32[4,2,512]{2,1,0:T(2,128)S(1)} %exponential_add_fusion, f32[4,2,512]{2,1,0:T(2,128)S(1)} %broadcast_maximum_fusion, f32[512,640]{0,1:T(8,128)S(1)} %fusion.18, ...), kind=kOutput, calls=%fused_computation.39 | convolution fusion | flops 354156544 | bytes 13008928 | tf_op jit(solution)/shard_map/kgqs,skd->qkgd/dot_general | solution.py:53
  186.0 1.3 copy.30
  187.9 35.7 %collective-permute-done.3 = bf16[512,2048]{1,0:T(8,128)(2,1)} collective-permute-done((bf16[512,2048]{1,0:T(8,128)(2,1)}, bf16[512,2048]{1,0:T(8,128)(2,1)}, u32[]{:S(2)}, u32[]{:S(2)}) %collective-permute-start.3) | collective-permute-done | bytes 2097184 | tf_op jit(solution)/shard_map/ppermute | solution.py:133
  223.6 5.2 %fusion.17 = bf16[1,512,2048]{2,1,0:T(8,128)(2,1)} fusion(bf16[512,2048]{1,0:T(8,128)(2,1)} %collective-permute-done.3, bf16[1024,2048]{1,0:T(8,128)(2,1)S(1)} %copy-done.14, bf16[512,512]{1,0:T(8,128)(2,1)S(1)} %fusion.26, bf16[512,512]{1,0:T(8,128)(2,1)S(1)} %copy.30), kind=kOutput, calls=%fused_computation.28 | convolution fusion | flops 2154823680 | bytes 9437184 | tf_op jit(solution)/shard_map/dot_general | solution.py:125
  (71 shorter events, 17.3 us)
Async XLA Ops:
  6.5 96.8 %all-gather.3.cloned.1.call-start = ((), (), s32[]{:S(2)}) async-start(), calls=%async_computation | async-start | bytes 11141120 | tf_op jit(solution)/shard_map/all_gather | solution.py:70
  10.1 11.9 %copy-start.8 = (bf16[1,1024,1024]{2,1,0:T(8,128)(2,1)S(1)}, bf16[1,1024,1024]{2,1,0:T(8,128)(2,1)}, u32[]{:S(2)}) copy-start(bf16[1,1024,1024]{2,1,0:T(8,128)(2,1)} %param.12) | copy-start | bytes 6291460
  12.1 0.8 copy-start.11
  12.9 143.9 %all-gather.5.cloned.1.call-start = ((), (), s32[]{:S(2)}) async-start(), calls=%async_computation.1 | async-start | bytes 4456448 | tf_op jit(solution)/shard_map/all_gather | solution.py:72
  13.0 49.0 %collective-permute-start = (bf16[1024,1024]{1,0:T(8,128)(2,1)}, bf16[1024,1024]{1,0:T(8,128)(2,1)}, u32[]{:S(2)}, u32[]{:S(2)}) collective-permute-start(bf16[1024,1024]{1,0:T(8,128)(2,1)} %bitcast.66), channel_id=1, source_target_pairs={{0,1},{1,0},{2,3},{3,2},{4,5},{5,4},{6,7},{7,6},{8,9},{9,8},{10,11... | collective-permute-start | bytes 6291464 | tf_op jit(solution)/shard_map/ppermute | solution.py:64
  63.8 2.0 copy-start
  63.8 39.5 %copy-start.15 = (f32[2048]{0:T(1024)S(1)}, f32[2048]{0:T(1024)}, u32[]{:S(2)}) copy-start(f32[2048]{0:T(1024)} %param.13) | copy-start | bytes 24580
  120.3 11.2 %collective-permute-start.2 = (bf16[2,512]{1,0:T(2,128)(2,1)}, bf16[2,512]{1,0:T(2,128)(2,1)}, u32[]{:S(2)}, u32[]{:S(2)}) collective-permute-start(bf16[2,512]{1,0:T(2,128)(2,1)} %slice.93), channel_id=1, source_target_pairs={{0,8},{8,16},{16,24},{1,9},{9,17},{17,25},{2,10},{10,18},{18,26},{... | collective-permute-start | bytes 6152 | tf_op jit(solution)/shard_map/ppermute | solution.py:14
  123.5 12.3 %collective-permute-start.1 = (bf16[128,512]{1,0:T(8,128)(2,1)}, bf16[128,512]{1,0:T(8,128)(2,1)S(1)}, u32[]{:S(2)}, u32[]{:S(2)}) collective-permute-start(bf16[128,512]{1,0:T(8,128)(2,1)} %slice.84), channel_id=1, source_target_pairs={{0,8},{8,16},{16,24},{1,9},{9,17},{17,25},{2,10},{10,18},{18,26},{... | collective-permute-start | bytes 393224 | tf_op jit(solution)/shard_map/ppermute | solution.py:14
  127.6 1.0 copy-start.4
  131.5 2.4 %copy-start.2 = (bf16[1024,512]{1,0:T(8,128)(2,1)S(1)}, bf16[1024,512]{1,0:T(8,128)(2,1)}, u32[]{:S(2)}) copy-start(bf16[1024,512]{1,0:T(8,128)(2,1)} %get-tuple-element.12) | copy-start | bytes 3145732
  133.8 6.0 %copy-start.10 = (pred[512,640]{0,1:T(8,128)(4,1)S(1)}, pred[512,640]{0,1:T(8,128)(4,1)}, u32[]{:S(2)}) copy-start(pred[512,640]{0,1:T(8,128)(4,1)} %get-tuple-element.26) | copy-start | bytes 983044
  144.1 3.0 %copy-start.12 = (bf16[640,256]{0,1:T(8,128)(2,1)S(1)}, bf16[640,256]{0,1:T(8,128)(2,1)}, u32[]{:S(2)}) copy-start(bf16[640,256]{0,1:T(8,128)(2,1)} %copy.21) | copy-start | bytes 983044
  153.3 9.7 %copy-start.5 = (bf16[1024,512]{1,0:T(8,128)(2,1)S(1)}, bf16[1024,512]{1,0:T(8,128)(2,1)}, u32[]{:S(2)}) copy-start(bf16[1024,512]{1,0:T(8,128)(2,1)} %copy-done.4) | copy-start | bytes 3145732
  153.3 12.6 %copy-start.6 = (bf16[1152,512]{1,0:T(8,128)(2,1)S(1)}, bf16[1152,512]{1,0:T(8,128)(2,1)}, u32[]{:S(2)}) copy-start(bf16[1152,512]{1,0:T(8,128)(2,1)} %pad_maximum_fusion) | copy-start | bytes 3538948
  166.1 4.5 %copy-start.9 = (pred[512,640]{0,1:T(8,128)(4,1)S(1)}, pred[512,640]{0,1:T(8,128)(4,1)}, u32[]{:S(2)}) copy-start(pred[512,640]{0,1:T(8,128)(4,1)} %get-tuple-element.25) | copy-start | bytes 983044
  170.5 4.0 %copy-start.1 = (f32[4,640,512,2]{2,1,3,0:T(8,128)}, f32[4,640,512,2]{2,1,3,0:T(8,128)S(1)}, u32[]{:S(2)}) copy-start(f32[4,640,512,2]{2,1,3,0:T(8,128)S(1)} %get-tuple-element.30) | copy-start | bytes 31457284
  175.5 48.1 %collective-permute-start.3 = (bf16[512,2048]{1,0:T(8,128)(2,1)}, bf16[512,2048]{1,0:T(8,128)(2,1)}, u32[]{:S(2)}, u32[]{:S(2)}) collective-permute-start(bf16[512,2048]{1,0:T(8,128)(2,1)} %convolution_convert_fusion.2), channel_id=1, source_target_pairs={{0,1},{1,0},{2,3},{3,2},{4,5},{5,4},{6,7},{7,6},{8,9},{9,8},{10,11... | collective-permute-start | bytes 6291464 | tf_op jit(solution)/shard_map/ppermute | solution.py:133
  177.0 10.3 %copy-start.7 = (bf16[1026,512]{1,0:T(8,128)(2,1)S(1)}, bf16[1026,512]{1,0:T(8,128)(2,1)}, u32[]{:S(2)}) copy-start(bf16[1026,512]{1,0:T(8,128)(2,1)} %pad_maximum_fusion.1) | copy-start | bytes 3151876
  177.0 10.5 %copy-start.3 = (bf16[1024,512]{1,0:T(8,128)(2,1)S(1)}, bf16[1024,512]{1,0:T(8,128)(2,1)}, u32[]{:S(2)}) copy-start(bf16[1024,512]{1,0:T(8,128)(2,1)} %get-tuple-element.12) | copy-start | bytes 3145732
  177.0 10.5 %copy-start.13 = (f32[1,512]{1,0:T(1,128)S(1)}, f32[1,512]{1,0:T(1,128)}, u32[]{:S(2)}) copy-start(f32[1,512]{1,0:T(1,128)} %get-tuple-element.24) | copy-start | bytes 6148
  187.3 36.3 %copy-start.14 = (bf16[1024,2048]{1,0:T(8,128)(2,1)S(1)}, bf16[1024,2048]{1,0:T(8,128)(2,1)}, u32[]{:S(2)}) copy-start(bf16[1024,2048]{1,0:T(8,128)(2,1)} %all-gather.5.cloned.1.call-done) | copy-start | bytes 12582916
Sparse Core Ops, SparseCore 0:
  13.0 90.2 all-gather.2
  105.5 51.2 all-gather.4
